TPU v7x, 512 devices: a whole 4x4x16 slice. The times are simulated.
512 devices in a mesh: gr: 2 (over z_hi), fs: 32 (over z_lo, y), tp: 8 (over x, core).
Axes of the slice: x: 4, y: 4, z: 16 (z_hi: 2, z_lo: 8; z = z_hi * 8 + z_lo), core: 2. Of those that a mesh axis runs over, the one named last changes fastest.
Arguments:
- tokens: bfloat16 [12288, 2048], P(('gr', 'fs')), may hold values from -6 to 6
- routes: int32 [12288, 8], P(('gr', 'fs')), may hold values from 0 to 63, all different within a row; in each aligned block of 192 rows (0 to 191, 192 to 383, ...) at most 36 rows name the same one
- route_weight: float32 [12288, 8], P(('gr', 'fs')), may hold values from 0.05 to 0.6
- norm_gain: float32 [2048], replicated, may hold values from 0.1 to 1.9
- gate_experts: float32 [2, 32, 512, 2048], P('gr', None, 'fs', 'tp'), may hold values from -0.125 to 0.125
- up_experts: float32 [2, 32, 512, 2048], P('gr', None, 'fs', 'tp'), may hold values from -0.125 to 0.125
- down_experts: float32 [2, 32, 512, 2048], P('gr', None, 'fs', 'tp'), may hold values from -0.25 to 0.25
- gate_shared: float32 [2048, 512], P('fs', 'tp'), may hold values from -0.125 to 0.125
- up_shared: float32 [2048, 512], P('fs', 'tp'), may hold values from -0.125 to 0.125
- down_shared: float32 [512, 2048], P('fs', 'tp'), may hold values from -0.25 to 0.25
Outputs:
- mixed: bfloat16 [12288, 2048], P(('gr', 'fs'), 'tp')
- gate_served: bfloat16 [2, 32, 512, 2048], P(None, 'fs', 'tp')
- up_served: bfloat16 [2, 32, 512, 2048], P(None, 'fs', 'tp')
- down_served: bfloat16 [2, 32, 512, 2048], P(None, 'fs', None, 'tp')
- gate_shared_served: bfloat16 [2048, 512], P(None, 'tp')
- up_shared_served: bfloat16 [2048, 512], P(None, 'tp')
- down_shared_served: bfloat16 [512, 2048], P(None, 'tp')
Inputs may be any that keep to these rules, and one draw needn't show every extreme that they name: `routes`: each row names 8 different experts; within the 192 rows of one device no expert is named by more than 36 rows, and some expert reaches 36.
All inputs are finite; a program needn't handle non-finite values.
Results may differ from a plain program's by a relative error of at most 0.0084.
Values may be sent and summed in bfloat16 or wider, within the bound.
No kernel may reach another device: no remote copies, remote signals or barrier semaphores. Data moves between devices by JAX's collectives and lax.ppermute only.
A program may use at most 128 MiB of HBM per device.

v0:
```python
import jax
import jax.numpy as jnp
from jax import lax
from jax.sharding import PartitionSpec as P

EXP_HALF = 1
EPS = 1e-06


def sent_to_all(shard, axis):
    copies = jnp.broadcast_to(shard, (lax.axis_size(axis), *shard.shape))
    return lax.all_to_all(copies, axis, split_axis=0, concat_axis=0, tiled=True)


def joined_along(parts, dim):
    dims = list(parts.shape[1:])
    dims[dim] *= parts.shape[0]
    return jnp.moveaxis(parts, 0, dim).reshape(dims)


def collect(shard, axis, dim):
    parts = sent_to_all(shard, axis)
    return joined_along(parts, dim)


def side_by_side(arrays, axis, dim, along):
    widths = [a.shape[along] for a in arrays]
    both = jnp.concatenate(arrays, axis=along)
    whole = collect(both, axis, dim)
    return tuple(jnp.split(whole, [sum(widths[:k]) for k in range(1, len(widths))], axis=along))


def sent_together(arrays, axis, split_dim, concat_dim, along):
    widths = [a.shape[along] for a in arrays]
    both = jnp.concatenate(arrays, axis=along)
    whole = lax.all_to_all(both, axis, split_axis=split_dim, concat_axis=concat_dim, tiled=True)
    return tuple(jnp.split(whole, [sum(widths[:k]) for k in range(1, len(widths))], axis=along))


def in_one_piece(arrays, axis, dim, along):
    both = jnp.concatenate(arrays, axis=along)
    whole, at, gathered = (lax.all_gather(both, axis, axis=dim, tiled=True), 0, [])
    for a in arrays:
        gathered.append(lax.slice_in_dim(whole, at, at + a.shape[along], axis=along))
        at += a.shape[along]
    return tuple(gathered)


def on_device(
    tokens,
    routes,
    route_weight,
    norm_gain,
    gate_experts,
    up_experts,
    down_experts,
    gate_shared,
    up_shared,
    down_shared,
):
    bf = jnp.bfloat16
    f32 = jnp.float32
    n_fs = lax.axis_size("fs")
    n_gr = lax.axis_size("gr")
    n_tp = lax.axis_size("tp")
    fs_index = lax.axis_index("fs")
    cols_here = gate_experts.shape[3]
    gain_cols = lax.dynamic_slice_in_dim(norm_gain, lax.axis_index("tp") * cols_here, cols_here, 0)
    gate_local = (gate_experts * gain_cols[None, None, None, :]).astype(bf)
    up_local = (up_experts * gain_cols[None, None, None, :]).astype(bf)
    down_local = down_experts.astype(bf)
    shared_here = gate_shared.shape[0]
    gain_shared = lax.dynamic_slice_in_dim(norm_gain, fs_index * shared_here, shared_here, 0)
    gate_sh_local = (gate_shared * gain_shared[:, None]).astype(bf)
    up_sh_local = (up_shared * gain_shared[:, None]).astype(bf)
    down_sh_local = down_shared.astype(bf)
    halves = side_by_side((gate_local, up_local, down_local), "gr", 0, 1)
    gate_cols, up_cols, down_w = sent_together((halves[0], halves[1], halves[2]), "fs", 1, 2, 0)
    gate_w, up_w = sent_together((gate_cols, up_cols), "tp", 2, 3, 0)
    gate_sw, up_sw, down_sw = (
        *in_one_piece((gate_sh_local, up_sh_local), "fs", 0, 1),
        lax.all_gather(down_sh_local, "fs", axis=0, tiled=True),
    )
    values = tokens.astype(f32)
    normed = (values * lax.rsqrt(jnp.mean(values * values, axis=-1, keepdims=True) + EPS)).astype(
        bf
    )
    tok_count, top = routes.shape
    width = tokens.shape[1]
    per_group = gate_experts.shape[1]
    count = per_group * n_gr
    capacity = (3 * tok_count * top + 2 * count - 1) // (2 * count)
    flat_e = routes.reshape(-1)
    onehot = (flat_e[:, None] == jnp.arange(count, dtype=jnp.int32)[None, :]).astype(jnp.int32)
    ranks = jnp.sum(jnp.cumsum(onehot, axis=0) * onehot, axis=1) - 1
    group_of = flat_e // per_group
    within = flat_e % per_group
    target = within // EXP_HALF
    local_k = within % EXP_HALF
    slot = ((target * n_gr + group_of) * EXP_HALF + local_k) * capacity + ranks
    total_slots = n_fs * n_gr * EXP_HALF * capacity
    repeated = jnp.repeat(normed, top, axis=0)
    send = jnp.zeros((total_slots, width), bf).at[slot].set(repeated)
    send = send.reshape(n_fs, n_gr, EXP_HALF, capacity, width)
    cols = width // n_tp
    send = lax.dynamic_slice_in_dim(send, lax.axis_index("tp") * cols, cols, 4)
    received = lax.all_to_all(send, "fs", split_axis=0, concat_axis=0, tiled=True)
    received = lax.all_gather(received, "tp", axis=4, tiled=True)
    gate = jnp.einsum("sgkcd,gkfd->sgkcf", received, gate_w, preferred_element_type=f32)
    upper = jnp.einsum("sgkcd,gkfd->sgkcf", received, up_w, preferred_element_type=f32)
    hidden = (jax.nn.silu(gate) * upper).astype(bf)
    full_hidden = collect(hidden, "tp", 4)
    result = jnp.einsum(
        "sgkcf,gkfe->sgkce", full_hidden, down_w, preferred_element_type=f32
    ).astype(bf)
    returned = lax.all_to_all(result, "fs", split_axis=0, concat_axis=0, tiled=True)
    picked = returned.reshape(total_slots, cols)[slot].reshape(tok_count, top, cols)
    routed = jnp.einsum("tkc,tk->tc", picked.astype(f32), route_weight)
    shared_gate = jnp.dot(normed, gate_sw, preferred_element_type=f32)
    shared_up = jnp.dot(normed, up_sw, preferred_element_type=f32)
    shared_hidden = (jax.nn.silu(shared_gate) * shared_up).astype(bf)
    shared_full = collect(shared_hidden, "tp", 1)
    shared = jnp.dot(shared_full, down_sw, preferred_element_type=f32)
    mixed = (routed + shared).astype(bf)
    return (mixed, gate_w, up_w, down_w, gate_sw, up_sw, down_sw)


def solution(mesh):
    return jax.shard_map(
        on_device,
        mesh=mesh,
        in_specs=(
            P(("gr", "fs"), None),
            P(("gr", "fs"), None),
            P(("gr", "fs"), None),
            P(),
            P("gr", None, "fs", "tp"),
            P("gr", None, "fs", "tp"),
            P("gr", None, "fs", "tp"),
            P("fs", "tp"),
            P("fs", "tp"),
            P("fs", "tp"),
        ),
        out_specs=(
            P(("gr", "fs"), "tp"),
            P(None, "fs", "tp", None),
            P(None, "fs", "tp", None),
            P(None, "fs", None, "tp"),
            P(None, "tp"),
            P(None, "tp"),
            P(None, "tp"),
        ),
        check_vma=False,
    )
```

profile of v0, /device:TPU:1, one launch (start us, length us, event | category | flops | bytes accessed | tf_op | source)
XLA Modules:
  0.0 694.6 jit_solution(2489082165161462181)
XLA Ops:
  7.2 0.9 copy.80
  8.4 1.4 fusion.8
  10.1 18.1 %reduce-window.6 = s32[64,12,128]{2,1,0:T(8,128)S(1)} reduce-window(s32[64,12,128]{2,1,0:T(8,128)S(1)} %fusion.32, s32[]{:T(128)} %constant.70.clone.1), window={size=1x1x128 pad=0_0x0_0x127_0}, to_apply=%region_0.0 | reduce-window | flops 12484608 | bytes 786436 | tf_op jit(solution)/shard_map/reduce-window
  29.3 14.6 %scatter_custom_fusion = bf16[2304,2048]{1,0:T(8,128)(2,1)} fusion(s32[1536]{0:T(1024)S(1)} %fusion.35, bf16[]{:T(256)} %constant.72.clone.1, bf16[192,2048]{1,0:T(8,128)(2,1)S(1)} %fusion.9), kind=kCustom, calls=%fused_computation.6 | custom fusion | bytes 10223618 | tf_op jit(solution)/shard_map/scatter | solution.py:103
  43.9 13.1 %reshape.234 = bf16[32,2,1,36,2048]{4,3,1,0,2:T(8,128)(2,1)} reshape(bf16[2304,2048]{1,0:T(8,128)(2,1)} %scatter_custom_fusion) | data formatting | bytes 18874368 | tf_op jit(solution)/shard_map/reshape | solution.py:104
  57.0 1.4 constant_dynamic-slice_fusion
  58.4 0.9 copy.85
  59.3 73.5 %all_to_all.49 = bf16[32,2,1,36,256]{4,1,3,2,0:T(2,128)(2,1)S(1)} all-to-all(bf16[32,2,1,36,256]{4,1,3,2,0:T(2,128)(2,1)S(1)} %copy.85), channel_id=1, replica_groups=mesh['gr'=2,'fs'=32,'tp'=8] {'fs'}, dimensions={0} | all-to-all | bytes 2359296 | tf_op jit(solution)/shard_map/all_to_all | solution.py:107
  132.8 1.3 copy.86
  134.1 0.8 dynamic_slice.9
  135.6 42.3 %all_to_all.50 = bf16[2,1,96,16,256]{4,3,2,1,0:T(8,128)(2,1)S(1)} all-to-all(bf16[2,1,96,16,256]{4,3,2,1,0:T(8,128)(2,1)S(1)} %broadcast_in_dim.10), channel_id=1, replica_groups=mesh['gr'=2,'fs'=32,'tp'=8] {'gr'}, dimensions={0} | all-to-all | bytes 3145728 | tf_op jit(solution)/shard_map/all_to_all | solution.py:12
  178.3 122.1 %all_to_all.51 = bf16[6,32,16,256]{3,2,0,1:T(8,128)(2,1)S(1)} all-to-all(bf16[6,32,16,256]{3,2,0,1:T(8,128)(2,1)S(1)} %copy.73), channel_id=1, replica_groups=mesh['gr'=2,'fs'=32,'tp'=8] {'fs'}, dimensions={1} | all-to-all | bytes 3145728 | tf_op jit(solution)/shard_map/all_to_all | solution.py:36
  300.8 0.8 copy.77
  301.6 21.3 %all_to_all.52 = bf16[4,1,512,256]{3,0,1,2:T(4,128)(2,1)S(1)} all-to-all(bf16[4,1,512,256]{3,0,1,2:T(4,128)(2,1)S(1)} %copy.77), channel_id=1, replica_groups=mesh['gr'=2,'fs'=32,'tp'=8] {'tp'}, dimensions={2} | all-to-all | bytes 2097152 | tf_op jit(solution)/shard_map/all_to_all | solution.py:36
  323.0 1.0 slice_bitcast_fusion
  324.3 1.0 reshape.257
  325.7 1.0 reshape.258
  326.7 5.9 fusion.11
  332.6 1.5 copy-done.12
  334.0 3.2 fusion.23
  337.4 3.0 broadcast_bitcast_fusion
  340.4 7.9 %reshape.268 = bf16[8,2,73728]{2,1,0:T(2,128)(2,1)} reshape(bf16[8,1,2,36,32,64]{5,4,3,2,1,0:T(8,128)(2,1)} %broadcast_bitcast_fusion) | data formatting | bytes 4718592
  348.3 5.3 all-to-all-start.4
  353.7 29.1 %all-to-all-done.4 = bf16[8,2,73728]{2,1,0:T(2,128)(2,1)} async-done(((bf16[8,2,73728]{2,1,0:T(2,128)(2,1)}), bf16[8,2,73728]{2,1,0:T(2,128)(2,1)}, u32[]{:S(2)}, u32[]{:S(2)}) %all-to-all-start.4) | async-done | bytes 2359328 | tf_op jit(solution)/shard_map/all_to_all | solution.py:12
  382.8 7.7 %reshape.269 = bf16[8,1,2,36,32,64]{5,4,3,2,1,0:T(8,128)(2,1)} reshape(bf16[8,2,73728]{2,1,0:T(2,128)(2,1)} %all-to-all-done.4) | data formatting | bytes 4718592
  390.5 3.1 bitcast_bitcast_fusion.1
  393.6 5.2 copy.105
  398.8 7.3 %reshape.264 = bf16[32,2,36,512]{3,2,0,1:T(8,128)(2,1)} reshape(bf16[32,2,1,36,8,64]{5,4,3,0,1,2:T(8,128)(2,1)} %copy.105) | data formatting | bytes 4718592 | tf_op jit(solution)/shard_map/reshape.37
  406.1 2.6 fusion.10
  408.7 2.2 copy.91
  410.9 5.6 all-to-all-start.5
  416.6 0.8 dynamic_slice.11
  417.7 120.1 %all_gather.10 = bf16[2048,128]{1,0:T(8,128)(2,1)S(1)} all-gather(bf16[64,128]{1,0:T(8,128)(2,1)S(1)} %pad_maximum_fusion.2), channel_id=1, replica_groups=mesh['gr'=2,'fs'=32,'tp'=8] {'fs'}, dimensions={0}, use_global_device_ids=true | all-gather | bytes 540672 | tf_op jit(solution)/shard_map/all_gather | solution.py:42
  537.8 1.1 fusion.43
  538.9 1.9 copy.98
  540.8 1.9 copy.99
  542.8 100.0 %all_gather.11 = bf16[512,256]{1,0:T(8,128)(2,1)S(1)} all-gather(bf16[16,256]{1,0:T(8,128)(2,1)S(1)} %convert_element_type.64), channel_id=1, replica_groups=mesh['gr'=2,'fs'=32,'tp'=8] {'fs'}, dimensions={0}, use_global_device_ids=true | all-gather | bytes 270336 | tf_op jit(solution)/shard_map/all_gather | solution.py:82
  642.8 0.4 fusion.39
  643.2 0.7 fusion.27
  643.9 0.8 copy.110
  644.8 0.8 copy.111
  645.6 0.8 broadcast_in_dim.27
  646.4 0.4 copy-done
  646.8 32.6 %all-to-all-start.6 = ((bf16[8,192,64]{1,2,0:T(8,128)(2,1)}), bf16[8,192,64]{1,2,0:T(8,128)(2,1)S(1)}, u32[]{:S(2)}, u32[]{:S(2)}) async-start(bf16[8,192,64]{1,2,0:T(8,128)(2,1)} %broadcast_in_dim.27), calls=%async_computation.6 | async-start | bytes 524288 | tf_op jit(solution)/shard_map/all_to_all | solution.py:12
  679.3 1.5 copy.92
  681.1 4.8 gather_fusion
  686.2 0.9 fusion.26
  687.1 0.7 copy.116
  (66 shorter events, 4.9 us)
Async XLA Ops:
  7.2 2.6 copy-start.1
  7.2 319.5 %all-gather.2.cloned.1.call-start = ((), (), s32[]{:S(2)}) async-start(), calls=%async_computation.7 | async-start | bytes 11796480 | tf_op jit(solution)/shard_map/all_gather | solution.py:108
  132.8 1.3 copy-start.3
  134.0 1.0 copy-start.6
  134.0 1.2 copy-start.7
  326.7 5.9 copy-start.5
  326.7 7.3 %copy-start.12 = (bf16[32,2,1,36,2048]{4,3,0,1,2:T(8,128)(2,1)S(1)}, bf16[32,2,1,36,2048]{4,3,0,1,2:T(8,128)(2,1)}, u32[]{:S(2)}) copy-start(bf16[32,2,1,36,2048]{4,3,0,1,2:T(8,128)(2,1)} %all-gather.2.cloned.1.call-done) | copy-start | bytes 28311556
  348.3 34.4 %all-to-all-start.4 = ((bf16[8,2,73728]{2,1,0:T(2,128)(2,1)}), bf16[8,2,73728]{2,1,0:T(2,128)(2,1)}, u32[]{:S(2)}, u32[]{:S(2)}) async-start(bf16[8,2,73728]{2,1,0:T(2,128)(2,1)} %reshape.268), calls=%async_computation.4 | async-start | bytes 4718592 | tf_op jit(solution)/shard_map/all_to_all | solution.py:12
  353.7 52.5 %copy-start.4 = (bf16[2,32,16,256]{3,2,1,0:T(8,128)(2,1)}, bf16[2,32,16,256]{3,2,1,0:T(8,128)(2,1)S(1)}, u32[]{:S(2)}) copy-start(bf16[2,32,16,256]{3,2,1,0:T(8,128)(2,1)S(1)} %copy.107) | copy-start | bytes 1572868
  410.9 6.4 copy-start.10
  410.9 6.4 copy-start.11
  410.9 6.6 copy-start.8
  410.9 6.6 copy-start.9
  410.9 234.7 %all-to-all-start.5 = ((bf16[32,2,1,36,256]{4,1,3,2,0:T(2,128)(2,1)}), bf16[32,2,1,36,256]{4,1,3,2,0:T(2,128)(2,1)S(1)}, u32[]{:S(2)}, u32[]{:S(2)}) async-start(bf16[32,2,1,36,256]{4,1,3,2,0:T(2,128)(2,1)} %copy.91), calls=%async_computation.5 | async-start | bytes 2359296 | tf_op jit(solution)/shard_map/all_to_all | solution.py:116
  542.8 101.1 %copy-start.2 = (bf16[1,2,8,8,8,256]{5,4,3,2,1,0:T(8,128)(2,1)S(1)}, bf16[1,2,8,8,8,256]{5,4,3,2,1,0:T(8,128)(2,1)}, u32[]{:S(2)}) copy-start(bf16[1,2,8,8,8,256]{5,4,3,2,1,0:T(8,128)(2,1)} %get-tuple-element.35) | copy-start | bytes 1572868
  645.6 1.1 copy-start
  646.8 39.4 %all-to-all-start.6 = ((bf16[8,192,64]{1,2,0:T(8,128)(2,1)}), bf16[8,192,64]{1,2,0:T(8,128)(2,1)S(1)}, u32[]{:S(2)}, u32[]{:S(2)}) async-start(bf16[8,192,64]{1,2,0:T(8,128)(2,1)} %broadcast_in_dim.27), calls=%async_computation.6 | async-start | bytes 524288 | tf_op jit(solution)/shard_map/all_to_all | solution.py:12
Sparse Core Ops, SparseCore 0:
  134.2 66.9 all-gather.1
where the time goes:
time: 696 us; the launch traced here: 695 us
  blocking collectives  479 us (69%)
  local copies, waits for them, and re-layouts  93.5 us (13%)
  starting transfers between devices  43.5 us (6%)
  waiting for transfers between devices  29.1 us (4%)
  other arithmetic  20.9 us (3%)
  between operations  14.4 us (2%)
  matrix products  14 us (2%)
    all_to_all x2, blocking collectives, sent_together(): lax.all_to_all(both, axis, split_axis=split_dim, concat_axis=concat_dim,...  143 us
    all_gather x1, blocking collectives, in_one_piece(): lax.all_gather(both, axis, axis=dim, tiled=True)  120 us
    all_gather x1, blocking collectives, on_device(): lax.all_gather(down_sh_local, 'fs', axis=0, tiled=True)  100 us
    all_to_all x1, blocking collectives, on_device(): lax.all_to_all(send, 'fs', split_axis=0, concat_axis=0, tiled=True)  73.5 us
    all_to_all x1, blocking collectives, sent_to_all(): return lax.all_to_all(copies, axis, split_axis=0, concat_axis=0, tiled=True)  42.3 us
    all_to_all x2, starting transfers between devices, sent_to_all(): return lax.all_to_all(copies, axis, split_axis=0, concat_axis=0, tiled=True)  37.9 us
    all_to_all x2, waiting for transfers between devices, sent_to_all(): return lax.all_to_all(copies, axis, split_axis=0, concat_axis=0, tiled=True)  29.1 us
    unnamed x38, local copies, waits for them, and re-layouts  27.5 us
  transfers between devices with their start and end apart: 4, of which 1 were waited for; matrix products, arithmetic and copies ran while one was open for 3% of the time, Pallas kernels for 0%

commit v1 on v0

--- a/solution.py
+++ b/solution.py
@@ -79,7 +79,9 @@
     gate_w, up_w = sent_together((gate_cols, up_cols), "tp", 2, 3, 0)
     gate_sw, up_sw, down_sw = (
         *in_one_piece((gate_sh_local, up_sh_local), "fs", 0, 1),
-        lax.all_gather(down_sh_local, "fs", axis=0, tiled=True),
+        jnp.concatenate(
+            lax.all_to_all(jnp.stack([down_sh_local] * lax.axis_size("fs")), "fs", 0, 0), axis=0
+        ),
     )
     values = tokens.astype(f32)
     normed = (values * lax.rsqrt(jnp.mean(values * values, axis=-1, keepdims=True) + EPS)).astype(

time: 696 us -> 595 us (0.85)
  blocking collectives: 479 us -> 379 us
    all_gather x1 -> x0, blocking collectives: 100 us -> none  [on_device(): lax.all_gather(down_sh_local, 'fs', axis=0, tiled=True)]
    all_to_all x2, starting transfers between devices: 37.9 us -> 24 us  [sent_to_all(): return lax.all_to_all(copies, axis, split_axis=0, concat_axis=0, tiled=True)]
    another operation x5 -> x6, local copies, waits for them, and re-layouts: 14.7 us -> 15.3 us
  transfers between devices with their start and end apart: 4 -> 5, of which waited for: 1 -> 1; matrix products, arithmetic and copies ran while one was open for 3% -> 9% of each run, Pallas kernels for 0% -> 0%
where the time goes in v1:
time: 595 us; the launch traced here: 593 us
  blocking collectives  379 us (64%)
  local copies, waits for them, and re-layouts  94.3 us (16%)
  starting transfers between devices  41.7 us (7%)
  waiting for transfers between devices  29.2 us (5%)
  other arithmetic  20.9 us (4%)
  between operations  14.4 us (2%)
  matrix products  14 us (2%)
    all_to_all x2, blocking collectives, sent_together(): lax.all_to_all(both, axis, split_axis=split_dim, concat_axis=concat_dim,...  143 us
    all_gather x1, blocking collectives, in_one_piece(): lax.all_gather(both, axis, axis=dim, tiled=True)  119 us
    all_to_all x1, blocking collectives, on_device(): lax.all_to_all(send, 'fs', split_axis=0, concat_axis=0, tiled=True)  73.5 us
    all_to_all x1, blocking collectives, sent_to_all(): return lax.all_to_all(copies, axis, split_axis=0, concat_axis=0, tiled=True)  42.3 us
    all_to_all x2, waiting for transfers between devices, sent_to_all(): return lax.all_to_all(copies, axis, split_axis=0, concat_axis=0, tiled=True)  29.1 us
    unnamed x38, local copies, waits for them, and re-layouts  27.7 us
    all_to_all x2, starting transfers between devices, sent_to_all(): return lax.all_to_all(copies, axis, split_axis=0, concat_axis=0, tiled=True)  24 us
    another operation x3, other arithmetic  18.4 us
  transfers between devices with their start and end apart: 5, of which 1 were waited for; matrix products, arithmetic and copies ran while one was open for 9% of the time, Pallas kernels for 0%

profile of v1, /device:TPU:1, one launch (start us, length us, event | category | flops | bytes accessed | tf_op | source)
XLA Modules:
  0.0 593.1 jit_solution(2140871276625205075)
XLA Ops:
  7.2 0.9 copy.80
  8.4 1.4 fusion.8
  10.1 18.1 %reduce-window.6 = s32[64,12,128]{2,1,0:T(8,128)S(1)} reduce-window(s32[64,12,128]{2,1,0:T(8,128)S(1)} %fusion.32, s32[]{:T(128)} %constant.70.clone.1), window={size=1x1x128 pad=0_0x0_0x127_0}, to_apply=%region_0.0 | reduce-window | flops 12484608 | bytes 786436 | tf_op jit(solution)/shard_map/reduce-window
  29.3 14.6 %scatter_custom_fusion = bf16[2304,2048]{1,0:T(8,128)(2,1)} fusion(s32[1536]{0:T(1024)S(1)} %fusion.35, bf16[]{:T(256)} %constant.72.clone.1, bf16[192,2048]{1,0:T(8,128)(2,1)S(1)} %fusion.9), kind=kCustom, calls=%fused_computation.6 | custom fusion | bytes 10223618 | tf_op jit(solution)/shard_map/scatter | solution.py:105
  43.9 13.1 %reshape.239 = bf16[32,2,1,36,2048]{4,3,1,0,2:T(8,128)(2,1)} reshape(bf16[2304,2048]{1,0:T(8,128)(2,1)} %scatter_custom_fusion) | data formatting | bytes 18874368 | tf_op jit(solution)/shard_map/reshape | solution.py:106
  57.0 1.4 constant_dynamic-slice_fusion
  58.4 0.9 copy.85
  59.3 73.5 %all_to_all.54 = bf16[32,2,1,36,256]{4,1,3,2,0:T(2,128)(2,1)S(1)} all-to-all(bf16[32,2,1,36,256]{4,1,3,2,0:T(2,128)(2,1)S(1)} %copy.85), channel_id=1, replica_groups=mesh['gr'=2,'fs'=32,'tp'=8] {'fs'}, dimensions={0} | all-to-all | bytes 2359296 | tf_op jit(solution)/shard_map/all_to_all | solution.py:109
  132.8 1.3 copy.86
  134.1 0.8 dynamic_slice.9
  135.6 42.3 %all_to_all.55 = bf16[2,1,96,16,256]{4,3,2,1,0:T(8,128)(2,1)S(1)} all-to-all(bf16[2,1,96,16,256]{4,3,2,1,0:T(8,128)(2,1)S(1)} %broadcast_in_dim.10), channel_id=1, replica_groups=mesh['gr'=2,'fs'=32,'tp'=8] {'gr'}, dimensions={0} | all-to-all | bytes 3145728 | tf_op jit(solution)/shard_map/all_to_all | solution.py:12
  178.3 122.1 %all_to_all.56 = bf16[6,32,16,256]{3,2,0,1:T(8,128)(2,1)S(1)} all-to-all(bf16[6,32,16,256]{3,2,0,1:T(8,128)(2,1)S(1)} %copy.73), channel_id=1, replica_groups=mesh['gr'=2,'fs'=32,'tp'=8] {'fs'}, dimensions={1} | all-to-all | bytes 3145728 | tf_op jit(solution)/shard_map/all_to_all | solution.py:36
  300.8 0.8 copy.77
  301.6 21.3 %all_to_all.57 = bf16[4,1,512,256]{3,0,1,2:T(4,128)(2,1)S(1)} all-to-all(bf16[4,1,512,256]{3,0,1,2:T(4,128)(2,1)S(1)} %copy.77), channel_id=1, replica_groups=mesh['gr'=2,'fs'=32,'tp'=8] {'tp'}, dimensions={2} | all-to-all | bytes 2097152 | tf_op jit(solution)/shard_map/all_to_all | solution.py:36
  323.0 1.0 slice_bitcast_fusion
  324.3 1.0 reshape.263
  325.7 1.0 reshape.264
  326.7 5.9 fusion.11
  332.6 1.5 copy-done.12
  334.0 3.2 fusion.23
  337.4 3.0 broadcast_bitcast_fusion
  340.4 7.9 %reshape.274 = bf16[8,2,73728]{2,1,0:T(2,128)(2,1)} reshape(bf16[8,1,2,36,32,64]{5,4,3,2,1,0:T(8,128)(2,1)} %broadcast_bitcast_fusion) | data formatting | bytes 4718592
  348.3 5.4 all-to-all-start.4
  353.8 29.1 %all-to-all-done.4 = bf16[8,2,73728]{2,1,0:T(2,128)(2,1)} async-done(((bf16[8,2,73728]{2,1,0:T(2,128)(2,1)}), bf16[8,2,73728]{2,1,0:T(2,128)(2,1)}, u32[]{:S(2)}, u32[]{:S(2)}) %all-to-all-start.4) | async-done | bytes 2359328 | tf_op jit(solution)/shard_map/all_to_all | solution.py:12
  382.9 0.7 stack.2
  383.6 5.7 all-to-all-start.7
  389.4 7.9 %reshape.275 = bf16[8,1,2,36,32,64]{5,4,3,2,1,0:T(8,128)(2,1)} reshape(bf16[8,2,73728]{2,1,0:T(2,128)(2,1)} %all-to-all-done.4) | data formatting | bytes 4718592
  397.3 3.1 bitcast_bitcast_fusion.1
  400.4 5.2 copy.105
  405.6 7.3 %reshape.270 = bf16[32,2,36,512]{3,2,0,1:T(8,128)(2,1)} reshape(bf16[32,2,1,36,8,64]{5,4,3,0,1,2:T(8,128)(2,1)} %copy.105) | data formatting | bytes 4718592 | tf_op jit(solution)/shard_map/reshape.38
  412.9 2.6 fusion.10
  415.5 2.2 copy.91
  417.7 11.9 %all-to-all-start.5 = ((bf16[32,2,1,36,256]{4,1,3,2,0:T(2,128)(2,1)}), bf16[32,2,1,36,256]{4,1,3,2,0:T(2,128)(2,1)S(1)}, u32[]{:S(2)}, u32[]{:S(2)}) async-start(bf16[32,2,1,36,256]{4,1,3,2,0:T(2,128)(2,1)} %copy.91), calls=%async_computation.5 | async-start | bytes 2359296 | tf_op jit(solution)/shard_map/all_to_all | solution.py:118
  429.6 0.8 dynamic_slice.11
  430.8 119.5 %all_gather.7 = bf16[2048,128]{1,0:T(8,128)(2,1)S(1)} all-gather(bf16[64,128]{1,0:T(8,128)(2,1)S(1)} %pad_maximum_fusion.2), channel_id=1, replica_groups=mesh['gr'=2,'fs'=32,'tp'=8] {'fs'}, dimensions={0}, use_global_device_ids=true | all-gather | bytes 540672 | tf_op jit(solution)/shard_map/all_gather | solution.py:42
  550.2 1.1 fusion.43
  551.4 1.9 copy.98
  553.3 1.9 copy.99
  555.2 0.4 fusion.39
  555.6 0.7 fusion.27
  556.3 0.8 copy.110
  557.2 0.8 copy.111
  558.0 0.8 broadcast_in_dim.27
  559.2 18.6 %all-to-all-start.6 = ((bf16[8,192,64]{1,2,0:T(8,128)(2,1)}), bf16[8,192,64]{1,2,0:T(8,128)(2,1)S(1)}, u32[]{:S(2)}, u32[]{:S(2)}) async-start(bf16[8,192,64]{1,2,0:T(8,128)(2,1)} %broadcast_in_dim.27), calls=%async_computation.6 | async-start | bytes 524288 | tf_op jit(solution)/shard_map/all_to_all | solution.py:12
  577.8 1.5 copy.92
  579.5 4.8 gather_fusion
  584.6 0.9 fusion.26
  585.5 0.7 copy.116
  (68 shorter events, 5.2 us)
Async XLA Ops:
  7.2 2.6 copy-start.1
  7.2 319.5 %all-gather.2.cloned.1.call-start = ((), (), s32[]{:S(2)}) async-start(), calls=%async_computation.8 | async-start | bytes 11796480 | tf_op jit(solution)/shard_map/all_gather | solution.py:110
  132.8 1.3 copy-start.3
  134.0 1.0 copy-start.6
  134.0 1.2 copy-start.7
  326.7 5.9 copy-start.5
  326.7 7.3 %copy-start.12 = (bf16[32,2,1,36,2048]{4,3,0,1,2:T(8,128)(2,1)S(1)}, bf16[32,2,1,36,2048]{4,3,0,1,2:T(8,128)(2,1)}, u32[]{:S(2)}) copy-start(bf16[32,2,1,36,2048]{4,3,0,1,2:T(8,128)(2,1)} %all-gather.2.cloned.1.call-done) | copy-start | bytes 28311556
  348.3 5.4 copy-start.10
  348.3 34.6 %all-to-all-start.4 = ((bf16[8,2,73728]{2,1,0:T(2,128)(2,1)}), bf16[8,2,73728]{2,1,0:T(2,128)(2,1)}, u32[]{:S(2)}, u32[]{:S(2)}) async-start(bf16[8,2,73728]{2,1,0:T(2,128)(2,1)} %reshape.274), calls=%async_computation.4 | async-start | bytes 4718592 | tf_op jit(solution)/shard_map/all_to_all | solution.py:12
  383.6 34.1 %all-to-all-start.7 = ((bf16[32,16,256]{2,1,0:T(8,128)(2,1)}), bf16[32,16,256]{2,1,0:T(8,128)(2,1)S(1)}, u32[]{:S(2)}, u32[]{:S(2)}) async-start(bf16[32,16,256]{2,1,0:T(8,128)(2,1)} %stack.2), calls=%async_computation.7 | async-start | bytes 524288 | tf_op jit(solution)/shard_map/all_to_all | solution.py:83
  389.4 23.5 %copy-start.4 = (bf16[2,32,16,256]{3,2,1,0:T(8,128)(2,1)}, bf16[2,32,16,256]{3,2,1,0:T(8,128)(2,1)S(1)}, u32[]{:S(2)}) copy-start(bf16[2,32,16,256]{3,2,1,0:T(8,128)(2,1)S(1)} %copy.107) | copy-start | bytes 1572868
  417.7 12.7 %copy-start.11 = (f32[192,8]{0,1:T(8,128)S(1)}, f32[192,8]{0,1:T(8,128)}, u32[]{:S(2)}) copy-start(f32[192,8]{0,1:T(8,128)} %param.12) | copy-start | bytes 18436
  417.7 12.9 %copy-start.8 = (f32[64,64]{1,0:T(8,128)S(1)}, f32[64,64]{1,0:T(8,128)}, u32[]{:S(2)}) copy-start(f32[64,64]{1,0:T(8,128)} %param.17) | copy-start | bytes 49156
  417.7 12.9 %copy-start.9 = (f32[64,64]{1,0:T(8,128)S(1)}, f32[64,64]{1,0:T(8,128)}, u32[]{:S(2)}) copy-start(f32[64,64]{1,0:T(8,128)} %param.18) | copy-start | bytes 49156
  417.7 140.3 %all-to-all-start.5 = ((bf16[32,2,1,36,256]{4,1,3,2,0:T(2,128)(2,1)}), bf16[32,2,1,36,256]{4,1,3,2,0:T(2,128)(2,1)S(1)}, u32[]{:S(2)}, u32[]{:S(2)}) async-start(bf16[32,2,1,36,256]{4,1,3,2,0:T(2,128)(2,1)} %copy.91), calls=%async_computation.5 | async-start | bytes 2359296 | tf_op jit(solution)/shard_map/all_to_all | solution.py:118
  555.2 1.1 copy-start.2
  558.0 1.1 copy-start
  559.2 25.5 %all-to-all-start.6 = ((bf16[8,192,64]{1,2,0:T(8,128)(2,1)}), bf16[8,192,64]{1,2,0:T(8,128)(2,1)S(1)}, u32[]{:S(2)}, u32[]{:S(2)}) async-start(bf16[8,192,64]{1,2,0:T(8,128)(2,1)} %broadcast_in_dim.27), calls=%async_computation.6 | async-start | bytes 524288 | tf_op jit(solution)/shard_map/all_to_all | solution.py:12
Sparse Core Ops, SparseCore 0:
  134.2 66.9 all-gather.1
